TPU v7x, 32 devices: a whole 2x2x4 slice. The times are simulated.
32 devices in a mesh: sp: 4 (over y, x), tp: 8 (over z, core).
Axes of the slice: x: 2, y: 2, z: 4, core: 2. Of those that a mesh axis runs over, the one named last changes fastest.
Arguments:
- stream: bfloat16 [4096, 1024], P('tp', 'sp'), may hold values from -6 to 6
- value_weight: bfloat16 [2, 2048, 4096], P(None, 'tp', 'sp'), may hold values from -0.09375 to 0.09375
- gate_weight: bfloat16 [2, 2048, 4096], P(None, 'tp', 'sp'), may hold values from -0.09375 to 0.09375
- conv_taps: bfloat16 [2, 2048, 31], P(None, 'tp'), may hold values from -16 to 16
- norm_gain: bfloat16 [2, 2048], P(None, 'tp'), may hold values from 0.099609375 to 1.8984375
- out_weight: bfloat16 [2, 4096, 2048], P(None, 'tp', 'sp'), may hold values from -4 to 4
- out_gain: bfloat16 [2, 4096], P(None, 'tp'), may hold values from 0.099609375 to 1.8984375
Outputs:
- result: bfloat16 [4096, 1024], P('tp', 'sp')
All inputs are finite; a program needn't handle non-finite values.
Results may differ from a plain program's by a relative error of at most 0.015.
Values may be sent and summed in bfloat16 or wider, within the bound.
A program may use at most 64 MiB of HBM per device.

v0:
```python
import jax
import jax.numpy as jnp
from jax import lax
from jax.sharding import PartitionSpec as P

D = 4096
W = 2048
LAYERS = 2


def with_halo(cells, sides, width):
    for axis, dim in sides:
        count = lax.axis_size(axis)
        ends = count - 1
        head = lax.slice_in_dim(cells, 0, width, axis=dim)
        tail = lax.slice_in_dim(cells, cells.shape[dim] - width, cells.shape[dim], axis=dim)
        cells = jnp.concatenate(
            [
                lax.ppermute(tail, axis, [(i, (i + 1) % count) for i in range(ends)]),
                cells,
                lax.ppermute(head, axis, [((i + 1) % count, i) for i in range(ends)]),
            ],
            axis=dim,
        )
    return cells


def finish_layer(hidden, branch, feature_gain):
    branch_wide = lax.optimization_barrier(branch.astype(jnp.bfloat16)).astype(jnp.float32)
    square_total = lax.psum(jnp.sum(branch_wide * branch_wide, axis=0), "tp")
    factor = lax.rsqrt(square_total / D + 1e-06)
    return (hidden.astype(jnp.float32) + branch_wide * factor * feature_gain).astype(jnp.bfloat16)


def on_device(stream, value_weight, gate_weight, conv_taps, norm_gain, out_weight, out_gain):
    hidden = stream
    positions = hidden.shape[1]
    for layer_index in range(LAYERS):
        value_cols, gate_cols, out_cols = (
            lax.all_gather(value_weight[layer_index], "sp", axis=1, tiled=True),
            lax.all_gather(gate_weight[layer_index], "sp", axis=1, tiled=True),
            lax.all_gather(out_weight[layer_index], "sp", axis=1, tiled=True),
        )
        block_rows = lax.all_gather(hidden, "tp", axis=0, tiled=True)
        value_proj = jnp.dot(value_cols, block_rows, preferred_element_type=jnp.float32)
        gate_proj = jnp.dot(gate_cols, block_rows, preferred_element_type=jnp.float32)
        gated = (value_proj * jax.nn.sigmoid(gate_proj)).astype(jnp.bfloat16)
        kernel_taps = conv_taps[layer_index].astype(jnp.float32)
        reach = kernel_taps.shape[1] // 2
        padded = with_halo(gated, (("sp", 1),), reach).astype(jnp.float32)
        convolved = jnp.zeros(gated.shape, jnp.float32)
        for offset in range(kernel_taps.shape[1]):
            convolved = (
                convolved
                + kernel_taps[:, offset : offset + 1] * padded[:, offset : offset + positions]
            )
        conv_narrow = lax.optimization_barrier(convolved.astype(jnp.bfloat16))
        feature_gain = out_gain[layer_index].astype(jnp.float32)[:, None]
        conv_wide = conv_narrow.astype(jnp.float32)
        channel_totals = lax.psum(
            (jnp.sum(conv_wide, axis=0), jnp.sum(conv_wide * conv_wide, axis=0)), "tp"
        )
        average = channel_totals[0] / W
        variance = channel_totals[1] / W - average * average
        channel_gain = norm_gain[layer_index].astype(jnp.float32)[:, None]
        activated = jax.nn.silu(
            (conv_wide - average) * lax.rsqrt(variance + 1e-05) * channel_gain
        ).astype(jnp.bfloat16)
        branch = jnp.dot(
            out_cols,
            lax.all_gather(activated, "tp", axis=0, tiled=True),
            preferred_element_type=jnp.float32,
        )
        hidden = finish_layer(hidden, branch, feature_gain)
    return hidden


def solution(mesh):
    return jax.shard_map(
        on_device,
        mesh=mesh,
        in_specs=(
            P("tp", "sp"),
            P(None, "tp", "sp"),
            P(None, "tp", "sp"),
            P(None, "tp", None),
            P(None, "tp"),
            P(None, "tp", "sp"),
            P(None, "tp"),
        ),
        out_specs=P("tp", "sp"),
        check_vma=False,
    )
```

profile of v0, /device:TPU:0, one launch (start us, length us, event | category | flops | bytes accessed | tf_op | source)
XLA Modules:
  0.0 368.0 jit_solution(12427185381842521671)
XLA Ops:
  6.5 2.4 fusion.155
  8.9 0.0 all-gather.27.cloned.1.call-update
  8.9 0.0 all-gather.17.cloned.1.call-start
  9.0 0.7 all-gather.17.cloned.1.call-update
  9.7 0.0 all-gather.25.cloned.1.call-start
  9.7 1.0 fusion.154
  10.8 0.0 all-gather.25.cloned.1.call-update
  10.8 0.0 all-gather.29.cloned.1.call-start
  10.8 1.1 fusion.153
  11.9 0.0 all-gather.29.cloned.1.call-update
  11.9 0.0 all-gather.19.cloned.1.call-start
  12.1 35.0 %all-gather.27.cloned.1.call-done = bf16[1,256,4096]{2,1,0:T(8,128)(2,1)} async-done(((bf16[1,256,1024]{2,1,0:T(8,128)(2,1)}), bf16[1,256,4096]{2,1,0:T(8,128)(2,1)}) %all-gather.27.cloned.1.call-update) | async-done | bytes 2097168 | tf_op jit(solution)/shard_map/all_gather | solution.py:41
  47.1 30.8 %all-gather.17.cloned.1.call-done = bf16[4096,256]{1,0:T(8,128)(2,1)} async-done(((bf16[512,256]{1,0:T(8,128)(2,1)}), bf16[4096,256]{1,0:T(8,128)(2,1)}) %all-gather.17.cloned.1.call-update) | async-done | bytes 2097168 | tf_op jit(solution)/shard_map/all_gather | solution.py:44
  77.9 3.3 fusion.36
  81.2 0.0 copy-start.8
  81.2 33.1 %all-gather.25.cloned.1.call-done = bf16[1,256,4096]{2,1,0:T(8,128)(2,1)} async-done(((bf16[1,256,1024]{2,1,0:T(8,128)(2,1)}), bf16[1,256,4096]{2,1,0:T(8,128)(2,1)}) %all-gather.25.cloned.1.call-update) | async-done | bytes 2097168 | tf_op jit(solution)/shard_map/all_gather | solution.py:40
  114.4 2.5 fusion.57
  116.9 1.3 collective-permute-start.1
  118.2 4.5 %collective-permute-start = (bf16[256,15]{0,1:T(8,128)(2,1)S(1)}, bf16[256,15]{0,1:T(8,128)(2,1)S(1)}, u32[]{:S(2)}, u32[]{:S(2)}) collective-permute-start(bf16[256,15]{0,1:T(8,128)(2,1)S(1)} %get-tuple-element.21), channel_id=1, source_target_pairs={{0,8},{8,16},{16,24},{1,9},{9,17},{17,25},{2,10},{10,18},{18,26},{... | collective-permute-start | bytes 23048 | tf_op jit(solution)/shard_map/ppermute | solution.py:19
  122.8 0.0 collective-permute-done.1
  122.8 1.3 collective-permute-done
  124.1 0.0 copy-start.5
  124.1 0.0 copy-start.7
  124.2 0.7 fusion.121
  124.8 0.1 convert_reduce_fusion.1
  125.0 15.1 %all-reduce.1 = (f32[256]{0:T(256)S(1)}, f32[256]{0:T(256)S(1)}) all-reduce(f32[256]{0:T(256)S(1)} %get-tuple-element.8, f32[256]{0:T(256)S(1)} %get-tuple-element.7), channel_id=1, replica_groups=mesh['sp'=4,'tp'=8] {'tp'}, use_global_device_ids=true, to_apply=%region_3.0 | all-reduce | flops 512 | bytes 4096 | tf_op jit(solution)/shard_map/psum | solution.py:60
  140.1 0.8 fusion.78
  140.9 0.0 all-gather.19.cloned.1.call-update
  140.9 0.0 all-gather.33.cloned.1.call-start
  141.0 0.5 all-gather.33.cloned.1.call-update
  141.5 0.0 all-gather.21.cloned.1.call-start
  141.6 0.1 copy.12
  141.7 9.4 %all-gather.29.cloned.1.call-done = bf16[1,512,2048]{2,1,0:T(8,128)(2,1)} async-done(((bf16[1,512,512]{2,1,0:T(8,128)(2,1)}), bf16[1,512,2048]{2,1,0:T(8,128)(2,1)}) %all-gather.29.cloned.1.call-update) | async-done | bytes 2097168 | tf_op jit(solution)/shard_map/all_gather | solution.py:42
  151.1 25.3 %all-gather.19.cloned.1.call-done = bf16[2048,256]{0,1:T(8,128)(2,1)} async-done(((bf16[256,256]{0,1:T(8,128)(2,1)}), bf16[2048,256]{0,1:T(8,128)(2,1)}) %all-gather.19.cloned.1.call-update) | async-done | bytes 1048592 | tf_op jit(solution)/shard_map/all_gather | solution.py:71
  176.5 2.7 fusion.21
  179.1 0.1 fusion.63
  179.3 15.7 %psum.44 = f32[256]{0:T(256)S(1)} all-reduce(f32[256]{0:T(256)S(1)} %fusion.63), channel_id=1, replica_groups=mesh['sp'=4,'tp'=8] {'tp'}, use_global_device_ids=true, to_apply=%region_5.6 | all-reduce | flops 256 | bytes 2048 | tf_op jit(solution)/shard_map/psum | solution.py:30
  195.0 0.9 fusion.66
  195.9 0.0 all-gather.21.cloned.1.call-update
  195.9 0.0 all-gather.31.cloned.1.call-start
  196.0 0.7 all-gather.31.cloned.1.call-update
  196.7 0.0 all-gather.35.cloned.1.call-start
  196.7 0.7 all-gather.35.cloned.1.call-update
  197.4 0.0 all-gather.23.cloned.1.call-start
  197.5 14.7 %all-gather.33.cloned.1.call-done = bf16[1,256,4096]{2,1,0:T(8,128)(2,1)} async-done(((bf16[1,256,1024]{2,1,0:T(8,128)(2,1)}), bf16[1,256,4096]{2,1,0:T(8,128)(2,1)}) %all-gather.33.cloned.1.call-update) | async-done | bytes 2097168 | tf_op jit(solution)/shard_map/all_gather | solution.py:41
  212.1 30.8 %all-gather.21.cloned.1.call-done = bf16[4096,256]{0,1:T(8,128)(2,1)} async-done(((bf16[512,256]{0,1:T(8,128)(2,1)}), bf16[4096,256]{0,1:T(8,128)(2,1)}) %all-gather.21.cloned.1.call-update) | async-done | bytes 2097168 | tf_op jit(solution)/shard_map/all_gather | solution.py:44
  242.9 3.1 fusion.51
  246.0 33.3 %all-gather.31.cloned.1.call-done = bf16[1,256,4096]{2,1,0:T(8,128)(2,1)} async-done(((bf16[1,256,1024]{2,1,0:T(8,128)(2,1)}), bf16[1,256,4096]{2,1,0:T(8,128)(2,1)}) %all-gather.31.cloned.1.call-update) | async-done | bytes 2097168 | tf_op jit(solution)/shard_map/all_gather | solution.py:40
  279.4 2.3 fusion.60
  281.7 1.3 collective-permute-start.3
  283.0 4.5 %collective-permute-start.2 = (bf16[256,15]{0,1:T(8,128)(2,1)S(1)}, bf16[256,15]{0,1:T(8,128)(2,1)S(1)}, u32[]{:S(2)}, u32[]{:S(2)}) collective-permute-start(bf16[256,15]{0,1:T(8,128)(2,1)S(1)} %get-tuple-element.19), channel_id=1, source_target_pairs={{0,8},{8,16},{16,24},{1,9},{9,17},{17,25},{2,10},{10,18},{18,26},{... | collective-permute-start | bytes 23048 | tf_op jit(solution)/shard_map/ppermute | solution.py:19
  287.6 1.3 collective-permute-done.2
  289.0 0.7 fusion.90
  289.6 0.1 convert_reduce_fusion
  289.8 15.1 %all-reduce = (f32[256]{0:T(256)S(1)}, f32[256]{0:T(256)S(1)}) all-reduce(f32[256]{0:T(256)S(1)} %get-tuple-element.6, f32[256]{0:T(256)S(1)} %get-tuple-element.5), channel_id=1, replica_groups=mesh['sp'=4,'tp'=8] {'tp'}, use_global_device_ids=true, to_apply=%region_9.10 | all-reduce | flops 512 | bytes 4096 | tf_op jit(solution)/shard_map/psum | solution.py:60
  304.9 0.8 fusion.87
  305.7 0.0 all-gather.23.cloned.1.call-update
  305.7 10.5 %all-gather.35.cloned.1.call-done = bf16[1,512,2048]{2,1,0:T(8,128)(2,1)} async-done(((bf16[1,512,512]{2,1,0:T(8,128)(2,1)}), bf16[1,512,2048]{2,1,0:T(8,128)(2,1)}) %all-gather.35.cloned.1.call-update) | async-done | bytes 2097168 | tf_op jit(solution)/shard_map/all_gather | solution.py:42
  316.3 25.3 %all-gather.23.cloned.1.call-done = bf16[2048,256]{0,1:T(8,128)(2,1)} async-done(((bf16[256,256]{0,1:T(8,128)(2,1)}), bf16[2048,256]{0,1:T(8,128)(2,1)}) %all-gather.23.cloned.1.call-update) | async-done | bytes 1048592 | tf_op jit(solution)/shard_map/all_gather | solution.py:71
  341.6 2.7 fusion.18
  344.3 0.1 fusion.67
  344.4 15.7 %psum.47 = f32[256]{0:T(256)S(1)} all-reduce(f32[256]{0:T(256)S(1)} %fusion.67), channel_id=1, replica_groups=mesh['sp'=4,'tp'=8] {'tp'}, use_global_device_ids=true, to_apply=%region_11.12 | all-reduce | flops 256 | bytes 2048 | tf_op jit(solution)/shard_map/psum | solution.py:30
  360.2 0.2 fusion.70
  360.4 0.8 copy.17
  (33 shorter events, 0.3 us)
Async XLA Ops:
  6.5 3.2 copy-start.3
  6.5 40.6 %all-gather.27.cloned.1.call-start = ((), (), s32[]{:S(2)}) async-start(), calls=%async_computation.5 | async-start | bytes 2621440 | tf_op jit(solution)/shard_map/all_gather | solution.py:41
  8.9 1.9 copy-start.4
  8.9 69.0 %all-gather.17.cloned.1.call-start = ((), (), s32[]{:S(2)}) async-start(), calls=%async_computation | async-start | bytes 2359296 | tf_op jit(solution)/shard_map/all_gather | solution.py:44
  9.7 104.7 %all-gather.25.cloned.1.call-start = ((), (), s32[]{:S(2)}) async-start(), calls=%async_computation.4 | async-start | bytes 2621440 | tf_op jit(solution)/shard_map/all_gather | solution.py:40
  10.8 1.2 copy-start.6
  10.8 140.3 %all-gather.29.cloned.1.call-start = ((), (), s32[]{:S(2)}) async-start(), calls=%async_computation.6 | async-start | bytes 2621440 | tf_op jit(solution)/shard_map/all_gather | solution.py:42
  11.9 164.5 %all-gather.19.cloned.1.call-start = ((), (), s32[]{:S(2)}) async-start(), calls=%async_computation.1 | async-start | bytes 1179648 | tf_op jit(solution)/shard_map/all_gather | solution.py:71
  77.9 36.5 %copy-start.1 = (bf16[4096,256]{1,0:T(8,128)(2,1)S(1)}, bf16[4096,256]{1,0:T(8,128)(2,1)}, u32[]{:S(2)}) copy-start(bf16[4096,256]{1,0:T(8,128)(2,1)} %all-gather.17.cloned.1.call-done) | copy-start | bytes 6291460
  81.2 41.5 %copy-start.8 = (bf16[2,256]{1,0:T(2,128)(2,1)S(1)}, bf16[2,256]{1,0:T(2,128)(2,1)}, u32[]{:S(2)}) copy-start(bf16[2,256]{1,0:T(2,128)(2,1)} %param.11) | copy-start | bytes 3076
  116.9 5.9 %collective-permute-start.1 = (bf16[256,15]{0,1:T(8,128)(2,1)S(1)}, bf16[256,15]{0,1:T(8,128)(2,1)S(1)}, u32[]{:S(2)}, u32[]{:S(2)}) collective-permute-start(bf16[256,15]{0,1:T(8,128)(2,1)S(1)} %get-tuple-element.22), channel_id=1, source_target_pairs={{8,0},{16,8},{24,16},{9,1},{17,9},{25,17},{10,2},{18,10},{26,18},{... | collective-permute-start | bytes 23048 | tf_op jit(solution)/shard_map/ppermute | solution.py:21
  118.2 5.9 %collective-permute-start = (bf16[256,15]{0,1:T(8,128)(2,1)S(1)}, bf16[256,15]{0,1:T(8,128)(2,1)S(1)}, u32[]{:S(2)}, u32[]{:S(2)}) collective-permute-start(bf16[256,15]{0,1:T(8,128)(2,1)S(1)} %get-tuple-element.21), channel_id=1, source_target_pairs={{0,8},{8,16},{16,24},{1,9},{9,17},{17,25},{2,10},{10,18},{18,26},{... | collective-permute-start | bytes 23048 | tf_op jit(solution)/shard_map/ppermute | solution.py:19
  124.1 17.4 %copy-start.5 = (bf16[512,256]{1,0:T(8,128)(2,1)S(1)}, bf16[512,256]{1,0:T(8,128)(2,1)}, u32[]{:S(2)}) copy-start(bf16[512,256]{1,0:T(8,128)(2,1)} %param.7) | copy-start | bytes 786436
  124.1 17.6 %copy-start.7 = (bf16[2,512]{1,0:T(2,128)(2,1)S(1)}, bf16[2,512]{1,0:T(2,128)(2,1)}, u32[]{:S(2)}) copy-start(bf16[2,512]{1,0:T(2,128)(2,1)} %param.13) | copy-start | bytes 6148
  140.9 71.2 %all-gather.33.cloned.1.call-start = ((), (), s32[]{:S(2)}) async-start(), calls=%async_computation.8 | async-start | bytes 2621440 | tf_op jit(solution)/shard_map/all_gather | solution.py:41
  141.5 101.4 %all-gather.21.cloned.1.call-start = ((), (), s32[]{:S(2)}) async-start(), calls=%async_computation.2 | async-start | bytes 2359296 | tf_op jit(solution)/shard_map/all_gather | solution.py:44
  195.9 83.4 %all-gather.31.cloned.1.call-start = ((), (), s32[]{:S(2)}) async-start(), calls=%async_computation.7 | async-start | bytes 2621440 | tf_op jit(solution)/shard_map/all_gather | solution.py:40
  196.7 119.6 %all-gather.35.cloned.1.call-start = ((), (), s32[]{:S(2)}) async-start(), calls=%async_computation.9 | async-start | bytes 2621440 | tf_op jit(solution)/shard_map/all_gather | solution.py:42
  197.4 144.2 %all-gather.23.cloned.1.call-start = ((), (), s32[]{:S(2)}) async-start(), calls=%async_computation.3 | async-start | bytes 1179648 | tf_op jit(solution)/shard_map/all_gather | solution.py:71
  242.9 36.5 %copy-start.2 = (bf16[4096,256]{0,1:T(8,128)(2,1)S(1)}, bf16[4096,256]{0,1:T(8,128)(2,1)}, u32[]{:S(2)}) copy-start(bf16[4096,256]{0,1:T(8,128)(2,1)} %all-gather.21.cloned.1.call-done) | copy-start | bytes 6291460
  281.7 5.9 %collective-permute-start.3 = (bf16[256,15]{0,1:T(8,128)(2,1)S(1)}, bf16[256,15]{0,1:T(8,128)(2,1)S(1)}, u32[]{:S(2)}, u32[]{:S(2)}) collective-permute-start(bf16[256,15]{0,1:T(8,128)(2,1)S(1)} %get-tuple-element.20), channel_id=1, source_target_pairs={{8,0},{16,8},{24,16},{9,1},{17,9},{25,17},{10,2},{18,10},{26,18},{... | collective-permute-start | bytes 23048 | tf_op jit(solution)/shard_map/ppermute | solution.py:21
  283.0 5.9 %collective-permute-start.2 = (bf16[256,15]{0,1:T(8,128)(2,1)S(1)}, bf16[256,15]{0,1:T(8,128)(2,1)S(1)}, u32[]{:S(2)}, u32[]{:S(2)}) collective-permute-start(bf16[256,15]{0,1:T(8,128)(2,1)S(1)} %get-tuple-element.19), channel_id=1, source_target_pairs={{0,8},{8,16},{16,24},{1,9},{9,17},{17,25},{2,10},{10,18},{18,26},{... | collective-permute-start | bytes 23048 | tf_op jit(solution)/shard_map/ppermute | solution.py:19
  305.7 54.5 %copy-start = (bf16[512,256]{0,1:T(8,128)(2,1)S(1)}, bf16[512,256]{0,1:T(8,128)(2,1)}, u32[]{:S(2)}) copy-start(bf16[512,256]{0,1:T(8,128)(2,1)} %fusion.66) | copy-start | bytes 786436
Sparse Core Ops, SparseCore 0:
  9.2 37.8 all-gather.26
  48.7 29.1 all-gather.16
  79.7 34.5 all-gather.24
  116.0 35.0 all-gather.28
  152.5 23.8 all-gather.18
  178.2 33.9 all-gather.32
  213.7 29.1 all-gather.20
  244.8 34.5 all-gather.30
  281.2 35.0 all-gather.34
  317.7 23.8 all-gather.22
where the time goes:
time: 368 us
  waiting for transfers between devices  254 us (69%)
  blocking collectives  61.6 us (17%)
  matrix products  16.6 us (5%)
  between operations  13.8 us (4%)
  starting transfers between devices  12 us (3%)
  local copies, waits for them, and re-layouts  5.6 us (2%)
  other arithmetic  4.78 us (1%)
    all_gather x2, waiting for transfers between devices, on_device(): lax.all_gather(value_weight[layer_index], 'sp', axis=1, tiled=True)  66.4 us
    all_gather x2, waiting for transfers between devices, on_device(): block_rows = lax.all_gather(hidden, 'tp', axis=0, tiled=True)  61.6 us
    all_gather x2, waiting for transfers between devices, on_device(): lax.all_gather(activated, 'tp', axis=0, tiled=True)  50.7 us
    all_gather x2, waiting for transfers between devices, on_device(): lax.all_gather(gate_weight[layer_index], 'sp', axis=1, tiled=True)  49.7 us
    psum x2, blocking collectives, finish_layer(): square_total = lax.psum(jnp.sum(branch_wide * branch_wide, axis=0), 'tp')  31.5 us
    psum x2, blocking collectives, on_device(): lax.psum((jnp.sum(conv_wide, axis=0), jnp.sum(conv_wide * conv_wide, axis...  30.1 us
    all_gather x2, waiting for transfers between devices, on_device(): lax.all_gather(out_weight[layer_index], 'sp', axis=1, tiled=True)  19.9 us
    ppermute x2, starting transfers between devices, with_halo(): lax.ppermute(tail, axis, [(i, (i + 1) % count) for i in range(ends)])  9.09 us
  transfers between devices with their start and end apart: 14, of which 12 were waited for; matrix products, arithmetic and copies ran while one was open for 6% of the time, Pallas kernels for 0%

commit v1 on v0

v1 whole, which is shorter than its diff:
```python
import functools

import jax
import jax.numpy as jnp
from jax import lax
from jax.experimental import pallas as pl
from jax.experimental.pallas import tpu as pltpu
from jax.sharding import PartitionSpec as P

MESH = pl.DeviceIdType.MESH
F32 = jnp.float32
BF16 = jnp.bfloat16
LANES = 128
CONV_ROWS = 16


def grid_of(count):
    nx = int(count**0.5)
    while count % nx:
        nx -= 1
    return count // nx, nx


def kernel(
    n_sp, n_tp, n_layers,
    stream, value_w, gate_w, taps, norm_gain, out_w, out_gain,
    result,
    h_all, act_all, v_buf, g_buf, o_buf, gat, halo_l, halo_r, conv, acc, sums, squares,
    local_sem, send_sem, recv_sem,
):
    ny, nx = grid_of(n_sp)
    nz = n_tp // 2
    s, t = lax.axis_index("sp"), lax.axis_index("tp")
    y, x = s // nx, s % nx
    z, c = t // 2, t % 2
    features, positions = stream.shape
    channels = value_w.shape[1]
    f_cols = value_w.shape[2]
    c_cols = out_w.shape[2]
    width = channels * n_tp
    model = features * n_tp
    n_taps = taps.shape[2]
    reach = n_taps // 2
    counter = [0]
    sent = []

    def remote(src, dst, sp, tp):
        i = counter[0]
        counter[0] += 1
        return pltpu.make_async_remote_copy(
            src_ref=src, dst_ref=dst, send_sem=send_sem.at[i], recv_sem=recv_sem.at[i],
            device_id={"sp": sp, "tp": tp}, device_id_type=MESH,
        )

    def start(copy):
        copy.start()
        sent.append(copy)

    def slot_of(k, j):
        return lax.rem(y + ny - k, ny) * nx + lax.rem(x + nx - j, nx)

    def x_peer(j):
        return y * nx + lax.rem(x + j, nx)

    def y_peer(k):
        return lax.rem(y + k, ny) * nx + x

    class Gather:
        def __init__(self, src, dst, x_first):
            self.copies = {}
            for k in range(ny):
                for j in range(nx):
                    if k == 0 and j == 0:
                        continue
                    if x_first:
                        along_x = k == 0
                        origin = (0, 0) if along_x else (0, j)
                    else:
                        along_x = j > 0
                        origin = (k, 0) if along_x else (0, 0)
                    own = origin == (0, 0)
                    target = x_peer(j) if along_x else y_peer(k)
                    origin_slot = slot_of(*origin)
                    self.copies[k, j] = (
                        remote(src if own else dst(origin_slot), dst(origin_slot), target, t),
                        own, origin,
                    )
            i = local_count[0]
            local_count[0] += 1
            self.local = pltpu.make_async_copy(src, dst(s), local_sem.at[i])
            self.here = set()

        def start_own(self):
            for copy, own, _ in self.copies.values():
                if own:
                    start(copy)
            self.local.start()

        def forward(self):
            for copy, own, origin in self.copies.values():
                if not own:
                    self.arrive(*origin)
                    start(copy)

        def arrive(self, k, j):
            if (k, j) not in self.here:
                self.here.add((k, j))
                if k == 0 and j == 0:
                    self.local.wait()
                else:
                    self.copies[k, j][0].wait_recv()

    local_count = [0]

    class Spread:
        def __init__(self, buf, rows, src):
            def place(zz, cc):
                return buf.at[pl.ds(pl.multiple_of((zz * 2 + cc) * rows, rows), rows), :]

            self.along = {
                k: remote(src, place(z, c), s, lax.rem(z + k, nz) * 2 + c) for k in range(1, nz)
            }
            self.across = {0: remote(src, place(z, c), s, z * 2 + 1 - c)}
            for k in range(1, nz):
                back = lax.rem(z + nz - k, nz)
                self.across[k] = remote(place(back, c), place(back, c), s, z * 2 + 1 - c)

        def start_own(self):
            for k in self.order():
                start(self.along[k])
            start(self.across[0])

        def order(self):
            return sorted(self.along, key=lambda k: min(k, nz - k))

        def finish(self):
            for k in self.order():
                self.along[k].wait_recv()
                start(self.across[k])
            for k in self.across:
                self.across[k].wait_recv()

    def totals(buf):
        copies = []
        for k in range(1, n_tp):
            copies.append(remote(buf.at[t], buf.at[t], s, lax.rem(t + k, n_tp)))
            start(copies[-1])
        for copy in copies:
            copy.wait_recv()
        return jnp.sum(buf[...], axis=0)

    barrier = pltpu.get_barrier_semaphore()
    for k in range(1, n_sp):
        pl.semaphore_signal(
            barrier, inc=1, device_id={"sp": lax.rem(s + k, n_sp), "tp": t}, device_id_type=MESH
        )
    for k in range(1, n_tp):
        pl.semaphore_signal(
            barrier, inc=1, device_id={"sp": s, "tp": lax.rem(t + k, n_tp)}, device_id_type=MESH
        )
    pl.semaphore_wait(barrier, n_sp + n_tp - 2)

    half = features // 2
    in_proj, out_proj = [], []
    for l in range(n_layers):
        in_proj.append((
            Gather(value_w.at[l], lambda q, l=l: v_buf.at[l, q], True),
            Gather(gate_w.at[l], lambda q, l=l: g_buf.at[l, q], False),
        ))
        out_proj.append((
            Gather(out_w.at[l, pl.ds(0, half)], lambda q, l=l: o_buf.at[l, q, pl.ds(0, half)], True),
            Gather(
                out_w.at[l, pl.ds(half, half)], lambda q, l=l: o_buf.at[l, q, pl.ds(half, half)], False
            ),
        ))

    my_rows = pl.ds(pl.multiple_of(t * features, features), features)
    my_channels = pl.ds(pl.multiple_of(t * channels, channels), channels)
    stream_copy = pltpu.make_async_copy(stream, h_all.at[0, my_rows, :], local_sem.at[4 * n_layers])
    stream_copy.start()
    spread = Spread(h_all.at[0], features, stream)
    spread.start_own()
    for gather in in_proj[0]:
        gather.start_own()
    steps = [(k, j) for k in range(ny) for j in range(nx)]
    right, left = lax.rem(s + 1, n_sp), lax.rem(s + n_sp - 1, n_sp)

    for l in range(n_layers):
        spread.finish()
        if l == 0:
            stream_copy.wait()
        for gather in in_proj[l]:
            gather.forward()
        for k, j in steps:
            slot = slot_of(k, j)
            rows = pl.ds(pl.multiple_of(slot * f_cols, f_cols), f_cols)
            for half_index, (gather, buf) in enumerate(zip(in_proj[l], (v_buf, g_buf))):
                gather.arrive(k, j)
                part = jnp.dot(buf[l, slot], h_all[l, rows, :], preferred_element_type=F32)
                if (k, j) == (0, 0):
                    acc[half_index] = part
                else:
                    acc[half_index] += part
        gat[l] = (acc[0] * jax.nn.sigmoid(acc[1])).astype(BF16)

        to_right = remote(gat.at[l, :, pl.ds(positions - LANES, LANES)], halo_l.at[l], right, t)
        to_left = remote(gat.at[l, :, pl.ds(0, LANES)], halo_r.at[l], left, t)

        @pl.when(s < n_sp - 1)
        def _():
            to_right.start()

        @pl.when(s > 0)
        def _():
            to_left.start()

        for gather in out_proj[l]:
            gather.start_own()

        @pl.when(s == 0)
        def _():
            halo_l[l] = jnp.zeros_like(halo_l[l])

        @pl.when(s == n_sp - 1)
        def _():
            halo_r[l] = jnp.zeros_like(halo_r[l])

        @pl.when(s > 0)
        def _():
            to_right.wait_recv()

        @pl.when(s < n_sp - 1)
        def _():
            to_left.wait_recv()

        def conv_step(i, carry):
            rows = pl.ds(pl.multiple_of(i * CONV_ROWS, CONV_ROWS), CONV_ROWS)
            wide = jnp.concatenate(
                [halo_l[l, rows, :].astype(F32), gat[l, rows, :].astype(F32), halo_r[l, rows, :].astype(F32)],
                axis=1,
            )
            extent = wide.shape[1]
            weights = taps[l, rows, :].astype(F32)
            total = jnp.zeros((CONV_ROWS, positions), F32)
            for offset in range(n_taps):
                moved = pltpu.roll(wide, (reach - offset) % extent, 1)
                total = total + weights[:, offset : offset + 1] * moved[:, LANES : LANES + positions]
            narrow = total.astype(BF16)
            conv[rows, :] = narrow
            value = narrow.astype(F32)
            return (
                carry[0] + jnp.sum(value, axis=0, keepdims=True),
                carry[1] + jnp.sum(value * value, axis=0, keepdims=True),
            )

        zero = jnp.zeros((1, positions), F32)
        own_sum, own_square = lax.fori_loop(0, channels // CONV_ROWS, conv_step, (zero, zero))
        sums[l, t, 0:1, :] = own_sum
        sums[l, t, 1:2, :] = own_square
        channel_totals = totals(sums.at[l])
        average = channel_totals[0:1] / width
        variance = channel_totals[1:2] / width - average * average
        scaled = (conv[...].astype(F32) - average) * lax.rsqrt(variance + 1e-05) * norm_gain[l].astype(F32)
        act_all[l, my_channels, :] = (scaled / (1.0 + jnp.exp(-scaled))).astype(BF16)
        act_spread = Spread(act_all.at[l], channels, act_all.at[l, my_channels, :])
        act_spread.start_own()
        act_spread.finish()
        for gather in out_proj[l]:
            gather.forward()
        if l + 1 < n_layers:
            for gather in in_proj[l + 1]:
                gather.start_own()
        total = None
        for k, j in steps:
            slot = slot_of(k, j)
            rows = pl.ds(pl.multiple_of(slot * c_cols, c_cols), c_cols)
            for gather in out_proj[l]:
                gather.arrive(k, j)
            part = jnp.dot(o_buf[l, slot], act_all[l, rows, :], preferred_element_type=F32)
            total = part if total is None else total + part
        branch = total.astype(BF16).astype(F32)
        squares[l, t, 0:1, :] = jnp.sum(branch * branch, axis=0, keepdims=True)
        square_total = totals(squares.at[l])[0:1]
        factor = lax.rsqrt(square_total / model + 1e-06)
        fresh = h_all[l, my_rows, :].astype(F32) + branch * factor * out_gain[l].astype(F32)
        if l + 1 < n_layers:
            h_all[l + 1, my_rows, :] = fresh.astype(BF16)
            spread = Spread(h_all.at[l + 1], features, h_all.at[l + 1, my_rows, :])
            spread.start_own()
        else:
            result[...] = fresh.astype(BF16)

        @pl.when(s < n_sp - 1)
        def _():
            to_right.wait_send()

        @pl.when(s > 0)
        def _():
            to_left.wait_send()

    for copy in sent:
        copy.wait_send()


def on_device(n_sp, n_tp, stream, value_weight, gate_weight, conv_taps, norm_gain, out_weight, out_gain):
    layers, channels, f_cols = value_weight.shape
    features, positions = stream.shape
    c_cols = out_weight.shape[2]
    copies = layers * (4 * (n_sp - 1) + 2 + 4 * (n_tp - 1))
    vmem = pl.BlockSpec(memory_space=pltpu.VMEM)
    hbm = pl.BlockSpec(memory_space=pl.ANY)
    return pl.pallas_call(
        functools.partial(kernel, n_sp, n_tp, layers),
        out_shape=jax.ShapeDtypeStruct(stream.shape, BF16),
        in_specs=[hbm, hbm, hbm, vmem, vmem, hbm, vmem],
        out_specs=vmem,
        scratch_shapes=[
            pltpu.VMEM((layers, n_tp * features, positions), BF16),
            pltpu.VMEM((layers, n_tp * channels, positions), BF16),
            pltpu.VMEM((layers, n_sp, channels, f_cols), BF16),
            pltpu.VMEM((layers, n_sp, channels, f_cols), BF16),
            pltpu.VMEM((layers, n_sp, features, c_cols), BF16),
            pltpu.VMEM((layers, channels, positions), BF16),
            pltpu.VMEM((layers, channels, LANES), BF16),
            pltpu.VMEM((layers, channels, LANES), BF16),
            pltpu.VMEM((channels, positions), BF16),
            pltpu.VMEM((2, channels, positions), F32),
            pltpu.VMEM((layers, n_tp, 2, positions), F32),
            pltpu.VMEM((layers, n_tp, 1, positions), F32),
            pltpu.SemaphoreType.DMA((4 * layers + 1,)),
            pltpu.SemaphoreType.DMA((copies,)),
            pltpu.SemaphoreType.DMA((copies,)),
        ],
        compiler_params=pltpu.CompilerParams(
            collective_id=0, has_side_effects=True, vmem_limit_bytes=48 * 1024 * 1024
        ),
    )(stream, value_weight, gate_weight, conv_taps, norm_gain[:, :, None], out_weight, out_gain[:, :, None])


def solution(mesh):
    return jax.shard_map(
        functools.partial(on_device, mesh.shape["sp"], mesh.shape["tp"]),
        mesh=mesh,
        in_specs=(
            P("tp", "sp"),
            P(None, "tp", "sp"),
            P(None, "tp", "sp"),
            P(None, "tp", None),
            P(None, "tp"),
            P(None, "tp", "sp"),
            P(None, "tp"),
        ),
        out_specs=P("tp", "sp"),
        check_vma=False,
    )
```

time: 368 us -> 171 us (0.46)
  waiting for transfers between devices: 254 us -> 0 us
  Pallas kernels: 0 us -> 164 us
  blocking collectives: 61.6 us -> 0 us
  matrix products: 16.6 us -> 0 us
  between operations: 13.8 us -> 0.05 us
  starting transfers between devices: 12 us -> 0 us
  other arithmetic: 4.78 us -> 0 us
    all_gather x10 -> x0, waiting for transfers between devices: 248 us -> none  [the longest x2 66.4 us: on_device(): lax.all_gather(value_weight[layer_index], 'sp', axis=1, tiled=True)]
    pallas_call x0 -> x1, Pallas kernels: none -> 164 us  [on_device(): pl.pallas_call(functools.partial(kernel, n_sp, n_tp, layers), out_shape=j...]
    psum x4 -> x0, blocking collectives: 61.6 us -> none  [the longest x2 31.5 us: finish_layer(): square_total = lax.psum(jnp.sum(branch_wide * branch_wide, axis=0), 'tp')]
    dot_general x6 -> x0, matrix products: 16.6 us -> none  [the longest x2 6.44 us: on_device(): jnp.dot(gate_cols, block_rows, preferred_element_type=jnp.float32)]
    ppermute x4 -> x0, starting transfers between devices: 11.7 us -> none  [the longest x2 9.09 us: with_halo(): lax.ppermute(tail, axis, [(i, (i + 1) % count) for i in range(ends)])]
    unnamed x19 -> x14, local copies, waits for them, and re-layouts: 0.18 us -> 5.82 us
    slice x10 -> x0, local copies, waits for them, and re-layouts: 4.57 us -> none  [the longest x1 2.36 us: on_device(): gate_weight[layer_index]]
    convert_element_type x11 -> x0, other arithmetic: 4.19 us -> none  [the longest x2 1.69 us: on_device(): activated = jax.nn.silu((conv_wide - average) * lax.rsqrt(variance + 1e-0...]
  transfers between devices with their start and end apart: 14 -> 0, of which waited for: 12 -> 0; matrix products, arithmetic and copies ran while one was open for 6% -> 0% of each run, Pallas kernels for 0% -> 0%
where the time goes in v1:
time: 171 us; the launch traced here: 170 us
  Pallas kernels  164 us (96%)
  local copies, waits for them, and re-layouts  6.21 us (4%)
    pallas_call x1, Pallas kernels, on_device(): pl.pallas_call(functools.partial(kernel, n_sp, n_tp, layers), out_shape=j...  164 us
    unnamed x14, local copies, waits for them, and re-layouts  5.82 us

profile of v1, /device:TPU:0, one launch (start us, length us, event | category | flops | bytes accessed | tf_op | source)
XLA Modules:
  0.0 170.5 jit_solution(14045095655195894564)
XLA Ops:
  0.0 0.0 copy-start.5
  0.0 0.0 copy-start.3
  0.0 0.9 copy.9.taps
  1.0 0.0 copy-done.5
  1.0 0.0 copy-start.4
  1.0 0.2 copy.10.norm_gain
  1.2 0.5 copy-done.4
  1.6 0.2 copy.11.out_gain
  1.9 0.0 copy-done.3
  1.9 0.0 copy-start
  1.9 1.2 copy-done
  3.1 0.0 copy-start.1
  3.1 1.2 copy-done.1
  4.3 0.0 copy-start.2
  4.3 1.2 copy-done.2
  5.5 164.2 %shard_map.73 = bf16[512,256]{1,0:T(8,128)(2,1)S(1)} custom-call(bf16[512,256]{1,0:T(8,128)(2,1)S(1)} %copy-done.3, bf16[2,256,1024]{2,1,0:T(8,128)(2,1)S(1)} %copy-done, bf16[2,256,1024]{2,1,0:T(8,128)(2,1)S(1)} %copy-done.1, bf16[2,256,31]{2,1,0:T(8,128)(2,1)S(1)} %copy.9.taps, bf16[2,256,1]{2,1,0:T(8,128)(2,1)S(1)} %copy.10.norm_gain, ...), custom_call_target="tpu_custom_call" | custom-call | tf_op jit(solution)/shard_map/pallas_call | solution.py:312
  169.8 0.7 copy.13
Async XLA Ops:
  0.0 1.0 copy-start.5
  0.0 1.9 %copy-start.3 = (bf16[512,256]{1,0:T(8,128)(2,1)S(1)}, bf16[512,256]{1,0:T(8,128)(2,1)}, u32[]{:S(2)}) copy-start(bf16[512,256]{1,0:T(8,128)(2,1)} %stream.1) | copy-start | bytes 786436
  1.0 0.7 copy-start.4
  1.9 1.2 copy-start
  3.1 1.2 copy-start.1
  4.3 1.2 copy-start.2

commit v2 on v1

--- a/solution.py
+++ b/solution.py
@@ -52,9 +52,12 @@
             device_id={"sp": sp, "tp": tp}, device_id_type=MESH,
         )
 
-    def start(copy):
-        copy.start()
-        sent.append(copy)
+    def start(copy, condition=None):
+        if condition is None:
+            copy.start()
+        else:
+            pl.when(condition)(copy.start)
+        sent.append((copy, condition))
 
     def slot_of(k, j):
         return lax.rem(y + ny - k, ny) * nx + lax.rem(x + nx - j, nx)
@@ -68,6 +71,7 @@
     class Gather:
         def __init__(self, src, dst, x_first):
             self.copies = {}
+            self.x_first = x_first
             for k in range(ny):
                 for j in range(nx):
                     if k == 0 and j == 0:
@@ -90,11 +94,12 @@
             self.local = pltpu.make_async_copy(src, dst(s), local_sem.at[i])
             self.here = set()
 
-        def start_own(self):
-            for copy, own, _ in self.copies.values():
-                if own:
+        def start_own(self, first):
+            for (k, j), (copy, own, _) in self.copies.items():
+                if own and first == ((k == 0) == self.x_first):
                     start(copy)
-            self.local.start()
+            if first:
+                self.local.start()
 
         def forward(self):
             for copy, own, origin in self.copies.values():
@@ -112,33 +117,54 @@
 
     local_count = [0]
 
+    def start_pair(pair):
+        for first in (True, False):
+            for gather in pair:
+                gather.start_own(first)
+
+    def forward_pair(pair):
+        for gather in pair:
+            gather.forward()
+
     class Spread:
         def __init__(self, buf, rows, src):
             def place(zz, cc):
-                return buf.at[pl.ds(pl.multiple_of((zz * 2 + cc) * rows, rows), rows), :]
-
-            self.along = {
-                k: remote(src, place(z, c), s, lax.rem(z + k, nz) * 2 + c) for k in range(1, nz)
-            }
-            self.across = {0: remote(src, place(z, c), s, z * 2 + 1 - c)}
-            for k in range(1, nz):
-                back = lax.rem(z + nz - k, nz)
-                self.across[k] = remote(place(back, c), place(back, c), s, z * 2 + 1 - c)
+                row = pl.multiple_of((jnp.clip(zz, 0, nz - 1) * 2 + cc) * rows, rows)
+                return buf.at[pl.ds(row, rows), :]
+
+            self.across = remote(src, place(z, c), s, z * 2 + 1 - c)
+            self.along, self.hand, self.has = {}, {}, {}
+            for way in (1, -1):
+                after = jnp.clip(z + way, 0, nz - 1) * 2 + c
+                for d in range(1, nz):
+                    carried = z - way * (d - 1)
+                    origin = src if d == 1 else place(carried, c)
+                    self.along[way, d] = remote(origin, place(carried, c), s, after)
+                    self.has[way, d] = (z - way * d >= 0) & (z - way * d < nz)
+                    seen = place(z - way * d, c)
+                    self.hand[way, d] = remote(seen, seen, s, z * 2 + 1 - c)
+
+        def send(self, way, d):
+            holds = (z - way * (d - 1) >= 0) & (z - way * (d - 1) < nz)
+            more = (z + way >= 0) & (z + way < nz)
+            start(self.along[way, d], holds & more)
 
         def start_own(self):
-            for k in self.order():
-                start(self.along[k])
-            start(self.across[0])
-
-        def order(self):
-            return sorted(self.along, key=lambda k: min(k, nz - k))
+            for way in (1, -1):
+                self.send(way, 1)
+            start(self.across)
+
+        def step(self, d):
+            for way in (1, -1):
+                pl.when(self.has[way, d])(self.along[way, d].wait_recv)
+                if d + 1 < nz:
+                    self.send(way, d + 1)
+                start(self.hand[way, d], self.has[way, d])
 
         def finish(self):
-            for k in self.order():
-                self.along[k].wait_recv()
-                start(self.across[k])
-            for k in self.across:
-                self.across[k].wait_recv()
+            self.across.wait_recv()
+            for (way, d), hand in self.hand.items():
+                pl.when(self.has[way, d])(hand.wait_recv)
 
     def totals(buf):
         copies = []
@@ -180,17 +206,18 @@
     stream_copy.start()
     spread = Spread(h_all.at[0], features, stream)
     spread.start_own()
-    for gather in in_proj[0]:
-        gather.start_own()
+    start_pair(in_proj[0])
     steps = [(k, j) for k in range(ny) for j in range(nx)]
     right, left = lax.rem(s + 1, n_sp), lax.rem(s + n_sp - 1, n_sp)
 
     for l in range(n_layers):
+        for d in range(1, nz):
+            if d == nz - 1 and l == 0:
+                forward_pair(in_proj[0])
+            spread.step(d)
         spread.finish()
         if l == 0:
             stream_copy.wait()
-        for gather in in_proj[l]:
-            gather.forward()
         for k, j in steps:
             slot = slot_of(k, j)
             rows = pl.ds(pl.multiple_of(slot * f_cols, f_cols), f_cols)
@@ -214,8 +241,7 @@
         def _():
             to_left.start()
 
-        for gather in out_proj[l]:
-            gather.start_own()
+        start_pair(out_proj[l])
 
         @pl.when(s == 0)
         def _():
@@ -264,12 +290,12 @@
         act_all[l, my_channels, :] = (scaled / (1.0 + jnp.exp(-scaled))).astype(BF16)
         act_spread = Spread(act_all.at[l], channels, act_all.at[l, my_channels, :])
         act_spread.start_own()
+        forward_pair(out_proj[l])
+        if l + 1 < n_layers:
+            start_pair(in_proj[l + 1])
+        for d in range(1, nz):
+            act_spread.step(d)
         act_spread.finish()
-        for gather in out_proj[l]:
-            gather.forward()
-        if l + 1 < n_layers:
-            for gather in in_proj[l + 1]:
-                gather.start_own()
         total = None
         for k, j in steps:
             slot = slot_of(k, j)
@@ -287,6 +313,7 @@
             h_all[l + 1, my_rows, :] = fresh.astype(BF16)
             spread = Spread(h_all.at[l + 1], features, h_all.at[l + 1, my_rows, :])
             spread.start_own()
+            forward_pair(in_proj[l + 1])
         else:
             result[...] = fresh.astype(BF16)
 
@@ -298,15 +325,18 @@
         def _():
             to_left.wait_send()
 
-    for copy in sent:
-        copy.wait_send()
+    for copy, condition in sent:
+        if condition is None:
+            copy.wait_send()
+        else:
+            pl.when(condition)(copy.wait_send)
 
 
 def on_device(n_sp, n_tp, stream, value_weight, gate_weight, conv_taps, norm_gain, out_weight, out_gain):
     layers, channels, f_cols = value_weight.shape
     features, positions = stream.shape
     c_cols = out_weight.shape[2]
-    copies = layers * (4 * (n_sp - 1) + 2 + 4 * (n_tp - 1))
+    copies = layers * (4 * (n_sp - 1) + 2 + 2 * (n_tp - 1) + 2 * (4 * (n_tp // 2 - 1) + 1))
     vmem = pl.BlockSpec(memory_space=pltpu.VMEM)
     hbm = pl.BlockSpec(memory_space=pl.ANY)
     return pl.pallas_call(
@@ -332,7 +362,7 @@
             pltpu.SemaphoreType.DMA((copies,)),
         ],
         compiler_params=pltpu.CompilerParams(
-            collective_id=0, has_side_effects=True, vmem_limit_bytes=48 * 1024 * 1024
+            collective_id=0, has_side_effects=True, vmem_limit_bytes=60 * 1024 * 1024
         ),
     )(stream, value_weight, gate_weight, conv_taps, norm_gain[:, :, None], out_weight, out_gain[:, :, None])
 

time: 171 us -> 138 us (0.81)
  Pallas kernels: 164 us -> 133 us
    pallas_call x1, Pallas kernels: 164 us -> 133 us  [on_device(): pl.pallas_call(functools.partial(kernel, n_sp, n_tp, layers), out_shape=j...]
    unnamed x14 -> x6, local copies, waits for them, and re-layouts: 5.82 us -> 3.23 us
where the time goes in v2:
time: 138 us
  Pallas kernels  133 us (96%)
  local copies, waits for them, and re-layouts  4.92 us (4%)
    pallas_call x1, Pallas kernels, on_device(): pl.pallas_call(functools.partial(kernel, n_sp, n_tp, layers), out_shape=j...  133 us
    unnamed x6, local copies, waits for them, and re-layouts  3.23 us

profile of v2, /device:TPU:0, one launch (start us, length us, event | category | flops | bytes accessed | tf_op | source)
XLA Modules:
  0.0 138.2 jit_solution(12283359641941405594)
XLA Ops:
  0.0 0.0 copy-start.1
  0.0 1.6 %copy.9.taps = bf16[2,256,31]{2,1,0:T(8,128)(2,1)} copy(bf16[2,256,31]{1,0,2:T(2,128)(2,1)} %param.10) | data formatting | bytes 63488 | tf_op args[3]
  1.6 0.0 copy-done.1
  1.6 0.0 copy-start
  1.6 0.8 copy.10.norm_gain
  2.4 0.0 copy-done
  2.4 0.9 copy.11.out_gain
  3.2 133.3 %shard_map.73 = bf16[512,256]{1,0:T(8,128)(2,1)} custom-call(bf16[512,256]{1,0:T(8,128)(2,1)} %stream.1, bf16[2,256,1024]{2,1,0:T(8,128)(2,1)} %value_w.1, bf16[2,256,1024]{2,1,0:T(8,128)(2,1)} %gate_w.1, bf16[2,256,31]{2,1,0:T(8,128)(2,1)} %copy.9.taps, bf16[2,256,1]{2,1,0:T(8,128)(2,1)} %copy.10.norm_gain, bf16[2,512,512]{2,1,0:T(8,128)(2,1)} %out_w.1, ...), custom_call_target="tpu_custom_call" | custom-call | tf_op jit(solution)/shard_map/pallas_call | solution.py:342
  136.5 1.7 %copy.13 = bf16[512,256]{1,0:T(8,128)(2,1)} copy(bf16[512,256]{1,0:T(8,128)(2,1)} %shard_map.73) | data formatting | bytes 524288
Async XLA Ops:
  0.0 1.6 %copy-start.1 = (bf16[2,256]{1,0:T(2,128)(2,1)S(1)}, bf16[2,256]{1,0:T(2,128)(2,1)}, u32[]{:S(2)}) copy-start(bf16[2,256]{1,0:T(2,128)(2,1)} %param.11) | copy-start | bytes 3076
  1.6 0.8 copy-start

commit v3 on v2

--- a/solution.py
+++ b/solution.py
@@ -25,7 +25,8 @@
     n_sp, n_tp, n_layers,
     stream, value_w, gate_w, taps, norm_gain, out_w, out_gain,
     result,
-    h_all, act_all, v_buf, g_buf, o_buf, gat, halo_l, halo_r, conv, acc, sums, squares,
+    h_all, conv_all, branch_all, active, v_buf, g_buf, o_buf, gat, halo_l, halo_r, acc, sums, squares,
+    norm_rows, out_rows, norm_cols, out_cols,
     local_sem, send_sem, recv_sem,
 ):
     ny, nx = grid_of(n_sp)
@@ -166,14 +167,34 @@
             for (way, d), hand in self.hand.items():
                 pl.when(self.has[way, d])(hand.wait_recv)
 
-    def totals(buf):
+    def exchange(src, buf):
         copies = []
         for k in range(1, n_tp):
-            copies.append(remote(buf.at[t], buf.at[t], s, lax.rem(t + k, n_tp)))
+            copies.append(remote(src, buf.at[t], s, lax.rem(t + k, n_tp)))
             start(copies[-1])
+        return copies
+
+    def arrived(copies):
         for copy in copies:
             copy.wait_recv()
-        return jnp.sum(buf[...], axis=0)
+
+    def drain(spread, consume, between):
+        consume(t)
+        spread.across.wait_recv()
+        consume(z * 2 + 1 - c)
+        for d in range(1, nz):
+            spread.step(d)
+            if d == 1:
+                between()
+            for way in (1, -1):
+                @pl.when(spread.has[way, d])
+                def _():
+                    consume((z - way * d) * 2 + c)
+            for way in (1, -1):
+                @pl.when(spread.has[way, d])
+                def _():
+                    spread.hand[way, d].wait_recv()
+                    consume((z - way * d) * 2 + 1 - c)
 
     barrier = pltpu.get_barrier_semaphore()
     for k in range(1, n_sp):
@@ -207,17 +228,34 @@
     spread = Spread(h_all.at[0], features, stream)
     spread.start_own()
     start_pair(in_proj[0])
+    norm_rows[t] = norm_gain[...]
+    out_rows[t] = out_gain[...]
+    gain_copies = exchange(norm_gain, norm_rows) + exchange(out_gain, out_rows)
+
+    def to_columns(rows_ref, cols_ref, count):
+        def turn(i, carry):
+            rows = rows_ref[i].astype(F32)
+            fill = jnp.zeros((8 - n_layers, count), F32)
+            place = pl.ds(pl.multiple_of(i * count, count), count)
+            cols_ref[place, :] = jnp.concatenate([rows, fill], axis=0).T
+            return carry
+
+        lax.fori_loop(0, n_tp, turn, 0)
+
     steps = [(k, j) for k in range(ny) for j in range(nx)]
     right, left = lax.rem(s + 1, n_sp), lax.rem(s + n_sp - 1, n_sp)
 
     for l in range(n_layers):
-        for d in range(1, nz):
-            if d == nz - 1 and l == 0:
-                forward_pair(in_proj[0])
-            spread.step(d)
-        spread.finish()
         if l == 0:
+            for d in range(1, nz):
+                if d == nz - 1:
+                    forward_pair(in_proj[0])
+                spread.step(d)
+            spread.finish()
             stream_copy.wait()
+            arrived(gain_copies)
+            to_columns(norm_rows, norm_cols, channels)
+            to_columns(out_rows, out_cols, features)
         for k, j in steps:
             slot = slot_of(k, j)
             rows = pl.ds(pl.multiple_of(slot * f_cols, f_cols), f_cols)
@@ -272,7 +310,7 @@
                 moved = pltpu.roll(wide, (reach - offset) % extent, 1)
                 total = total + weights[:, offset : offset + 1] * moved[:, LANES : LANES + positions]
             narrow = total.astype(BF16)
-            conv[rows, :] = narrow
+            conv_all[l, pl.ds(pl.multiple_of(t * channels + i * CONV_ROWS, CONV_ROWS), CONV_ROWS), :] = narrow
             value = narrow.astype(F32)
             return (
                 carry[0] + jnp.sum(value, axis=0, keepdims=True),
@@ -283,39 +321,57 @@
         own_sum, own_square = lax.fori_loop(0, channels // CONV_ROWS, conv_step, (zero, zero))
         sums[l, t, 0:1, :] = own_sum
         sums[l, t, 1:2, :] = own_square
-        channel_totals = totals(sums.at[l])
-        average = channel_totals[0:1] / width
-        variance = channel_totals[1:2] / width - average * average
-        scaled = (conv[...].astype(F32) - average) * lax.rsqrt(variance + 1e-05) * norm_gain[l].astype(F32)
-        act_all[l, my_channels, :] = (scaled / (1.0 + jnp.exp(-scaled))).astype(BF16)
-        act_spread = Spread(act_all.at[l], channels, act_all.at[l, my_channels, :])
-        act_spread.start_own()
+        sum_copies = exchange(sums.at[l, t], sums.at[l])
+        conv_spread = Spread(conv_all.at[l], channels, conv_all.at[l, my_channels, :])
+        conv_spread.start_own()
         forward_pair(out_proj[l])
         if l + 1 < n_layers:
             start_pair(in_proj[l + 1])
-        for d in range(1, nz):
-            act_spread.step(d)
-        act_spread.finish()
+        arrived(sum_copies)
+        channel_totals = jnp.sum(sums[l], axis=0)
+        average = channel_totals[0:1] / width
+        variance = channel_totals[1:2] / width - average * average
+        inverse = lax.rsqrt(variance + 1e-05)
+
+        def activate(block):
+            rows = pl.ds(pl.multiple_of(block * channels, channels), channels)
+            gain = norm_cols[rows, l : l + 1]
+            scaled = (conv_all[l, rows, :].astype(F32) - average) * inverse * gain
+            active[rows, :] = (scaled / (1.0 + jnp.exp(-scaled))).astype(BF16)
+
+        drain(conv_spread, activate, lambda: None)
         total = None
         for k, j in steps:
             slot = slot_of(k, j)
             rows = pl.ds(pl.multiple_of(slot * c_cols, c_cols), c_cols)
             for gather in out_proj[l]:
                 gather.arrive(k, j)
-            part = jnp.dot(o_buf[l, slot], act_all[l, rows, :], preferred_element_type=F32)
+            part = jnp.dot(o_buf[l, slot], active[rows, :], preferred_element_type=F32)
             total = part if total is None else total + part
-        branch = total.astype(BF16).astype(F32)
+        narrow_branch = total.astype(BF16)
+        branch = narrow_branch.astype(F32)
         squares[l, t, 0:1, :] = jnp.sum(branch * branch, axis=0, keepdims=True)
-        square_total = totals(squares.at[l])[0:1]
-        factor = lax.rsqrt(square_total / model + 1e-06)
-        fresh = h_all[l, my_rows, :].astype(F32) + branch * factor * out_gain[l].astype(F32)
-        if l + 1 < n_layers:
-            h_all[l + 1, my_rows, :] = fresh.astype(BF16)
-            spread = Spread(h_all.at[l + 1], features, h_all.at[l + 1, my_rows, :])
+        square_copies = exchange(squares.at[l, t], squares.at[l])
+        last = l + 1 == n_layers
+        if not last:
+            branch_all[l, my_rows, :] = narrow_branch
+            spread = Spread(branch_all.at[l], features, branch_all.at[l, my_rows, :])
             spread.start_own()
-            forward_pair(in_proj[l + 1])
+        arrived(square_copies)
+        factor = lax.rsqrt(jnp.sum(squares[l], axis=0) / model + 1e-06)
+        if last:
+            gain = out_cols[my_rows, l : l + 1]
+            fresh = h_all[l, my_rows, :].astype(F32) + branch * factor * gain
+            result[...] = fresh.astype(BF16)
         else:
-            result[...] = fresh.astype(BF16)
+
+            def renew(block):
+                rows = pl.ds(pl.multiple_of(block * features, features), features)
+                gain = out_cols[rows, l : l + 1]
+                change = branch_all[l, rows, :].astype(F32) * factor * gain
+                h_all[l + 1, rows, :] = (h_all[l, rows, :].astype(F32) + change).astype(BF16)
+
+            drain(spread, renew, lambda: forward_pair(in_proj[l + 1]))
 
         @pl.when(s < n_sp - 1)
         def _():
@@ -336,7 +392,7 @@
     layers, channels, f_cols = value_weight.shape
     features, positions = stream.shape
     c_cols = out_weight.shape[2]
-    copies = layers * (4 * (n_sp - 1) + 2 + 2 * (n_tp - 1) + 2 * (4 * (n_tp // 2 - 1) + 1))
+    copies = layers * (4 * (n_sp - 1) + 2 + 2 * (n_tp - 1) + 2 * (4 * (n_tp // 2 - 1) + 1)) + 2 * (n_tp - 1)
     vmem = pl.BlockSpec(memory_space=pltpu.VMEM)
     hbm = pl.BlockSpec(memory_space=pl.ANY)
     return pl.pallas_call(
@@ -347,16 +403,21 @@
         scratch_shapes=[
             pltpu.VMEM((layers, n_tp * features, positions), BF16),
             pltpu.VMEM((layers, n_tp * channels, positions), BF16),
+            pltpu.VMEM((max(layers - 1, 1), n_tp * features, positions), BF16),
+            pltpu.VMEM((n_tp * channels, positions), BF16),
             pltpu.VMEM((layers, n_sp, channels, f_cols), BF16),
             pltpu.VMEM((layers, n_sp, channels, f_cols), BF16),
             pltpu.VMEM((layers, n_sp, features, c_cols), BF16),
             pltpu.VMEM((layers, channels, positions), BF16),
             pltpu.VMEM((layers, channels, LANES), BF16),
             pltpu.VMEM((layers, channels, LANES), BF16),
-            pltpu.VMEM((channels, positions), BF16),
             pltpu.VMEM((2, channels, positions), F32),
             pltpu.VMEM((layers, n_tp, 2, positions), F32),
             pltpu.VMEM((layers, n_tp, 1, positions), F32),
+            pltpu.VMEM((n_tp, layers, channels), BF16),
+            pltpu.VMEM((n_tp, layers, features), BF16),
+            pltpu.VMEM((n_tp * channels, 8), F32),
+            pltpu.VMEM((n_tp * features, 8), F32),
             pltpu.SemaphoreType.DMA((4 * layers + 1,)),
             pltpu.SemaphoreType.DMA((copies,)),
             pltpu.SemaphoreType.DMA((copies,)),
@@ -364,7 +425,7 @@
         compiler_params=pltpu.CompilerParams(
             collective_id=0, has_side_effects=True, vmem_limit_bytes=60 * 1024 * 1024
         ),
-    )(stream, value_weight, gate_weight, conv_taps, norm_gain[:, :, None], out_weight, out_gain[:, :, None])
+    )(stream, value_weight, gate_weight, conv_taps, norm_gain, out_weight, out_gain)
 
 
 def solution(mesh):

time: 138 us -> 131 us (0.949)
  Pallas kernels: 133 us -> 128 us
  local copies, waits for them, and re-layouts: 4.92 us -> 3.21 us
    pallas_call x1, Pallas kernels: 133 us -> 128 us  [on_device(): pl.pallas_call(functools.partial(kernel, n_sp, n_tp, layers), out_shape=j...]
    broadcast_in_dim x2 -> x0, local copies, waits for them, and re-layouts: 1.69 us -> none  [the longest x1 0.89 us: on_device(): out_gain[:, :, None]]
    unnamed x6 -> x2, local copies, waits for them, and re-layouts: 3.23 us -> 3.21 us
where the time goes in v3:
time: 131 us
  Pallas kernels  128 us (98%)
  local copies, waits for them, and re-layouts  3.21 us (2%)
    pallas_call x1, Pallas kernels, on_device(): pl.pallas_call(functools.partial(kernel, n_sp, n_tp, layers), out_shape=j...  128 us
    unnamed x2, local copies, waits for them, and re-layouts  3.21 us

profile of v3, /device:TPU:0, one launch (start us, length us, event | category | flops | bytes accessed | tf_op | source)
XLA Modules:
  0.0 131.2 jit_solution(8446631527920170012)
XLA Ops:
  0.0 1.5 %copy.8.taps = bf16[2,256,31]{2,1,0:T(8,128)(2,1)} copy(bf16[2,256,31]{1,0,2:T(2,128)(2,1)} %param.10) | data formatting | bytes 63488 | tf_op args[3]
  1.5 127.9 %shard_map.73 = bf16[512,256]{1,0:T(8,128)(2,1)} custom-call(bf16[512,256]{1,0:T(8,128)(2,1)} %stream.1, bf16[2,256,1024]{2,1,0:T(8,128)(2,1)} %value_w.1, bf16[2,256,1024]{2,1,0:T(8,128)(2,1)} %gate_w.1, bf16[2,256,31]{2,1,0:T(8,128)(2,1)} %copy.8.taps, bf16[2,256]{1,0:T(2,128)(2,1)} %norm_gain.1, bf16[2,512,512]{2,1,0:T(8,128)(2,1)} %out_w.1, ...), custom_call_target="tpu_custom_call" | custom-call | tf_op jit(solution)/shard_map/pallas_call | solution.py:398
  129.5 1.7 %copy.10 = bf16[512,256]{1,0:T(8,128)(2,1)} copy(bf16[512,256]{1,0:T(8,128)(2,1)} %shard_map.73) | data formatting | bytes 524288
